TPU v7x, 32 devices: a whole 2x2x4 slice. The times are simulated.
32 devices in a mesh: sp: 4 (over y, x), tp: 8 (over z, core).
Axes of the slice: x: 2, y: 2, z: 4, core: 2. Of those that a mesh axis runs over, the one named last changes fastest.
Arguments:
- saved_input: bfloat16 [1024, 2048], P('sp'), may hold values from -6 to 6
- cotangent: bfloat16 [1024, 2048], P('sp'), may hold values from -6 to 6
- expert_ids: int32 [1024, 2], P('sp'), may hold values from 0 to 3, all different within a row; in each aligned block of 256 rows (0 to 255, 256 to 511, ...) at most 256 rows name the same one
- route_weight: float32 [1024, 2], P('sp'), may hold values from 0.1 to 0.9
- w_gate: bfloat16 [4, 2048, 6144], P('sp', None, 'tp'), may hold values from -0.125 to 0.125
- w_up: bfloat16 [4, 2048, 6144], P('sp', None, 'tp'), may hold values from -0.125 to 0.125
- w_down: bfloat16 [4, 6144, 2048], P('sp', 'tp'), may hold values from -0.078125 to 0.078125
- w_out: bfloat16 [2048, 2048], P(None, 'tp'), may hold values from -0.125 to 0.125
- channel_gain: float32 [2048], P('tp'), may hold values from 0.1 to 1.9
- conv_taps: float32 [31, 2048], P(None, 'tp'), may hold values from -1 to 1
- glu_value: bfloat16 [2048, 1024], P('tp', 'sp'), may hold values from -6 to 6
- glu_gate: bfloat16 [2048, 1024], P('tp', 'sp'), may hold values from -8 to 8
- conv_out: bfloat16 [2048, 1024], P('tp', 'sp'), may hold values from -6 to 6
- norm_mean: float32 [1024], P('sp'), may hold values from -3 to 3
- norm_rstd: float32 [1024], P('sp'), may hold values from 0.5 to 2
Outputs:
- gate_grad: bfloat16 [4, 2048, 6144], P('sp', None, 'tp')
- up_grad: bfloat16 [4, 2048, 6144], P('sp', None, 'tp')
- down_grad: bfloat16 [4, 6144, 2048], P('sp', 'tp')
- proj_grad: float32 [2048, 2048], P('sp', 'tp')
- value_grad: bfloat16 [2048, 1024], P('tp', 'sp')
- gate_in_grad: bfloat16 [2048, 1024], P('tp', 'sp')
Inputs may be any that keep to these rules, and one draw needn't show every extreme that they name: `expert_ids`: the two experts of a position differ. In the positions of one block of 256, no expert is named more than 256 times, a bound that some block reaches.
All inputs are finite; a program needn't handle non-finite values.
Results may differ from a plain program's by a relative error of at most 0.018.
Values may be sent and summed in bfloat16 or wider, within the bound.
A program may use at most 128 MiB of HBM per device.

v0:
```python
import jax
import jax.numpy as jnp
from jax import lax
from jax.sharding import PartitionSpec as P

D = 2048
C = 2048


def from_behind(value, axis, by):
    devices = lax.axis_size(axis)
    pairs = [(i, i + by) for i in range(devices) if 0 <= i + by < devices]
    return lax.ppermute(value, axis, pairs)


def contract(left, right, left_dim, right_dim):
    return lax.dot_general(
        left, right, (((left_dim,), (right_dim,)), ((), ())), preferred_element_type=jnp.float32
    )


def expert_grads(rows_in, rows_cot, gate_weight, up_weight, down_weight):
    gate_pre = jnp.dot(rows_in, gate_weight, preferred_element_type=jnp.float32)
    up_pre = jnp.dot(rows_in, up_weight, preferred_element_type=jnp.float32)
    sigma = jax.nn.sigmoid(gate_pre)
    hidden = (gate_pre * sigma * up_pre).astype(jnp.bfloat16)
    hidden_cot = contract(rows_cot, down_weight, 1, 1)
    down_part = contract(hidden, rows_cot, 0, 0).astype(jnp.bfloat16)
    gate_cot = (hidden_cot * up_pre * sigma * (1.0 + gate_pre * (1.0 - sigma))).astype(jnp.bfloat16)
    up_cot = (hidden_cot * gate_pre * sigma).astype(jnp.bfloat16)
    gate_part = contract(rows_in, gate_cot, 0, 0).astype(jnp.bfloat16)
    up_part = contract(rows_in, up_cot, 0, 0).astype(jnp.bfloat16)
    input_cot = contract(gate_cot, gate_weight, 1, 1) + contract(up_cot, up_weight, 1, 1)
    return (gate_part, up_part, down_part, input_cot)


def on_device(
    saved_input,
    cotangent,
    expert_ids,
    route_weight,
    w_gate,
    w_up,
    w_down,
    w_out,
    channel_gain,
    conv_taps,
    glu_value,
    glu_gate,
    conv_out,
    norm_mean,
    norm_rstd,
):
    tokens_here = cotangent.shape[0]
    sp_count = lax.axis_size("sp")
    local_experts = w_gate.shape[0]
    expert_count = local_experts * sp_count
    capacity = 4 * tokens_here // expert_count
    pairs = expert_ids.reshape(2 * tokens_here)
    onehot = (pairs[:, None] == jnp.arange(expert_count, dtype=jnp.int32)[None, :]).astype(
        jnp.int32
    )
    before = jnp.cumsum(onehot, axis=0) - onehot
    target = pairs * capacity + jnp.sum(before * onehot, axis=1)
    owner = (
        jnp.zeros((expert_count * capacity,), jnp.int32)
        .at[target]
        .set(jnp.arange(2 * tokens_here, dtype=jnp.int32) + 1)
    )
    filled = (owner > 0)[:, None]
    pair_index = jnp.maximum(owner - 1, 0)
    scaled = (route_weight[:, :, None] * cotangent.astype(jnp.float32)[:, None, :]).astype(
        jnp.bfloat16
    )
    scaled = scaled.reshape(2 * tokens_here, D)
    send_cot = jnp.where(filled, scaled[pair_index], jnp.zeros_like(scaled[:1])).reshape(
        expert_count, capacity, D
    )
    send_in = jnp.where(filled, saved_input[pair_index // 2], jnp.zeros_like(saved_input[:1]))
    send_in = send_in.reshape(expert_count, capacity, D)
    rows_cot, rows_in = (
        lax.all_to_all(send_cot, "sp", split_axis=0, concat_axis=1, tiled=True),
        lax.all_to_all(send_in, "sp", split_axis=0, concat_axis=1, tiled=True),
    )
    results = [expert_grads(rows_in[0], rows_cot[0], w_gate[0], w_up[0], w_down[0])]
    gate_grad = jnp.stack([result[0] for result in results])
    up_grad = jnp.stack([result[1] for result in results])
    down_grad = jnp.stack([result[2] for result in results])
    input_cot = jnp.stack([result[3] for result in results])
    blocks = input_cot.reshape(local_experts, sp_count, capacity, D)
    share = lax.psum_scatter(
        blocks.astype(jnp.bfloat16), "tp", scatter_dimension=2, tiled=True
    ).astype(jnp.float32)
    returned = lax.all_to_all(
        share.astype(jnp.bfloat16), "sp", split_axis=1, concat_axis=0, tiled=True
    ).astype(share.dtype)
    whole = lax.all_gather(returned.astype(jnp.bfloat16), "tp", axis=2, tiled=True).astype(
        returned.dtype
    )
    routed = whole.reshape(expert_count * capacity, D)[target].reshape(tokens_here, 2, D)
    summed = jnp.sum(routed, axis=1)
    mixed_cot = (cotangent.astype(jnp.float32) + summed).astype(jnp.bfloat16)
    centered = (conv_out.astype(jnp.float32) - norm_mean[None, :]) * norm_rstd[None, :]
    normed = centered * channel_gain[:, None]
    sigma = jax.nn.sigmoid(normed)
    output_act = (normed * sigma).astype(jnp.bfloat16)
    proj_grad = lax.psum_scatter(
        contract(mixed_cot, output_act, 0, 1).astype(jnp.bfloat16),
        "sp",
        scatter_dimension=0,
        tiled=True,
    ).astype(jnp.float32)
    act_cot = contract(w_out, mixed_cot, 0, 1)
    norm_cot = act_cot * sigma * (1.0 + normed * (1.0 - sigma)) * channel_gain[:, None]
    first_sum, second_sum = lax.psum(
        (jnp.sum(norm_cot, axis=0), jnp.sum(norm_cot * centered, axis=0)), "tp"
    )
    conv_cot = norm_rstd[None, :] * (
        norm_cot - first_sum[None, :] / C - centered * second_sum[None, :] / C
    )
    reach = conv_taps.shape[0] - 1
    rim = from_behind(conv_cot[:, :reach], "sp", -1)
    padded = jnp.concatenate([conv_cot, rim], axis=1)
    glu_cot = conv_taps[0][:, None] * padded[:, :tokens_here]
    for lag in range(1, reach + 1):
        glu_cot = glu_cot + conv_taps[lag][:, None] * padded[:, lag : lag + tokens_here]
    gate_sigma = jax.nn.sigmoid(glu_gate.astype(jnp.float32))
    value_grad = (glu_cot * gate_sigma).astype(jnp.bfloat16)
    gate_in_grad = (
        glu_cot * glu_value.astype(jnp.float32) * gate_sigma * (1.0 - gate_sigma)
    ).astype(jnp.bfloat16)
    return (gate_grad, up_grad, down_grad, proj_grad, value_grad, gate_in_grad)


def solution(mesh):
    in_specs = (
        P("sp", None),
        P("sp", None),
        P("sp", None),
        P("sp", None),
        P("sp", None, "tp"),
        P("sp", None, "tp"),
        P("sp", "tp", None),
        P(None, "tp"),
        P("tp"),
        P(None, "tp"),
        P("tp", "sp"),
        P("tp", "sp"),
        P("tp", "sp"),
        P("sp"),
        P("sp"),
    )
    out_specs = (
        P("sp", None, "tp"),
        P("sp", None, "tp"),
        P("sp", "tp", None),
        P("sp", "tp"),
        P("tp", "sp"),
        P("tp", "sp"),
    )
    return jax.shard_map(
        on_device, mesh=mesh, in_specs=in_specs, out_specs=out_specs, check_vma=False
    )
```

profile of v0, /device:TPU:4, one launch (start us, length us, event | category | flops | bytes accessed | tf_op | source)
XLA Modules:
  0.0 370.3 jit_solution(1634541059612848329)
XLA Ops:
  9.5 1.2 reduce-window.6
  11.3 2.4 scatter_custom_fusion
  14.7 5.3 %mul.440 = f32[256,2,2048]{2,1,0:T(2,128)} broadcast(bf16[256,2048]{1,0:T(8,128)(2,1)} %param.16), dimensions={0,2} | broadcast | bytes 5242880 | tf_op jit(solution)/shard_map/mul | solution.py:72
  20.1 6.2 %mul.441 = f32[512,2048]{1,0:T(8,128)} reshape(f32[256,2,2048]{2,1,0:T(2,128)} %mul.440) | data formatting | bytes 8388608 | tf_op jit(solution)/shard_map/mul | solution.py:72
  26.2 10.2 %gather_fusion = bf16[1024,2048]{1,0:T(8,128)(2,1)} fusion(bf16[256,2048]{1,0:T(8,128)(2,1)} %param.15, s32[1024]{0:T(1024)S(1)} %get-tuple-element.64), kind=kCustom, calls=%fused_computation | custom fusion | bytes 8392704 | tf_op jit(solution)/shard_map/gather | solution.py:79
  36.4 3.8 %multiply_convert_fusion = bf16[512,2048]{1,0:T(8,128)(2,1)} fusion(f32[512,2048]{1,0:T(8,128)} %mul.441, f32[512]{0:T(512)S(1)} %mul.438), kind=kLoop, calls=%fused_computation.6 | loop fusion | flops 2097152 | bytes 6293504 | tf_op jit(solution)/shard_map/convert_element_type | solution.py:72
  40.2 10.7 %gather_fusion.1 = bf16[1024,2048]{1,0:T(8,128)(2,1)} fusion(bf16[512,2048]{1,0:T(8,128)(2,1)} %multiply_convert_fusion, s32[1024]{0:T(1024)S(1)} %get-tuple-element.63), kind=kCustom, calls=%fused_computation.1 | custom fusion | bytes 8392704 | tf_op jit(solution)/shard_map/gather | solution.py:76
  50.9 5.2 %broadcast_select_fusion = (bf16[4,256,2048]{2,1,0:T(8,128)(2,1)}, bf16[4,256,2048]{2,1,0:T(8,128)(2,1)S(1)}) fusion(bf16[4,256,2048]{2,1,0:T(8,128)(2,1)} %bitcast.104, pred[4,256]{1,0:T(4,128)(4,1)S(1)} %broadcast_in_dim.43, bf16[4,256,2048]{2,1,0:T(8,128)(2,1)} %bitcast.103), kind=kLoop, calls=%fused_computation.7 | loop fusion | flops 4194304 | bytes 16778240 | tf_op jit(solution)/shard_map/jit(_where)/select_n | solution.py:76
  56.1 50.8 %all_to_all.30 = bf16[4,256,2048]{2,1,0:T(8,128)(2,1)} all-to-all(bf16[4,256,2048]{2,1,0:T(8,128)(2,1)S(1)} %get-tuple-element.66), channel_id=1, replica_groups=mesh['sp'=4,'tp'=8] {'sp'}, dimensions={0} | all-to-all | bytes 8388608 | tf_op jit(solution)/shard_map/all_to_all | solution.py:83
  107.0 5.9 %all-to-all-start.1 = ((bf16[4,256,2048]{2,1,0:T(8,128)(2,1)}), bf16[4,256,2048]{2,1,0:T(8,128)(2,1)}, u32[]{:S(2)}, u32[]{:S(2)}) async-start(bf16[4,256,2048]{2,1,0:T(8,128)(2,1)} %get-tuple-element.65), calls=%async_computation.1 | async-start | bytes 8388608 | tf_op jit(solution)/shard_map/all_to_all | solution.py:82
  113.3 7.4 %fusion.2 = f32[1024,768]{1,0:T(8,128)} fusion(bf16[1024,2048]{1,0:T(8,128)(2,1)} %bitcast.105, bf16[1,2048,768]{2,1,0:T(8,128)(2,1)S(1)} %copy-done), kind=kOutput, calls=%fused_computation.43 | convolution fusion | flops 3221225472 | bytes 10485760 | tf_op jit(solution)/shard_map/dot_general | solution.py:23
  120.7 5.1 %fusion.5 = f32[1024,768]{1,0:T(8,128)} fusion(bf16[1024,2048]{1,0:T(8,128)(2,1)S(1)} %bitcast.108, bf16[1,2048,768]{2,1,0:T(8,128)(2,1)S(1)} %copy-done.41), kind=kOutput, calls=%fused_computation.46 | convolution fusion | flops 3221225472 | bytes 10485760 | tf_op jit(solution)/shard_map/dot_general | solution.py:24
  125.8 32.8 %all-to-all-done.1 = bf16[4,256,2048]{2,1,0:T(8,128)(2,1)} async-done(((bf16[4,256,2048]{2,1,0:T(8,128)(2,1)}), bf16[4,256,2048]{2,1,0:T(8,128)(2,1)}, u32[]{:S(2)}, u32[]{:S(2)}) %all-to-all-start.1) | async-done | bytes 4194336 | tf_op jit(solution)/shard_map/all_to_all | solution.py:82
  158.6 9.2 %multiply_convert_fusion.2 = (bf16[1024,768]{1,0:T(8,128)(2,1)S(1)}, bf16[1024,768]{1,0:T(8,128)(2,1)S(1)}) fusion(f32[1024,768]{1,0:T(8,128)} %fusion.2, f32[1024,768]{1,0:T(8,128)} %fusion.5, bf16[1024,2048]{1,0:T(8,128)(2,1)} %bitcast.6, bf16[1,768,2048]{2,1,0:T(8,128)(2,1)} %param.21), kind=kOutput, calls=%fused_computation.51 | convolution fusion | flops 3231449088 | bytes 16777216 | tf_op jit(solution)/shard_map/dot_general | solution.py:17
  167.8 3.4 fusion
  171.3 17.2 %add_convert_fusion = bf16[1024,2048]{1,0:T(8,128)(2,1)} fusion(f32[1024,2048]{1,0:T(8,128)S(1)} %fusion, bf16[1024,768]{1,0:T(8,128)(2,1)S(1)} %get-tuple-element.30, bf16[1,2048,768]{2,1,0:T(8,128)(2,1)S(1)} %copy-done.42), kind=kOutput, calls=%fused_computation.4 | convolution fusion | flops 3225419776 | bytes 17301504 | tf_op jit(solution)/shard_map/dot_general | solution.py:17
  188.5 50.3 %reduce-scatter.3.cloned.1.call-done = bf16[1,4,32,2048]{3,2,0,1:T(8,128)(2,1)} async-done(((bf16[1,4,256,2048]{3,2,0,1:T(8,128)(2,1)}), bf16[1,4,32,2048]{3,2,0,1:T(8,128)(2,1)}) %reduce-scatter.3.cloned.1.call-update) | async-done | bytes 524304 | tf_op jit(solution)/shard_map/reduce_scatter | solution.py:91
  238.8 10.8 %all_to_all.31 = bf16[1,4,32,2048]{3,2,0,1:T(8,128)(2,1)} all-to-all(bf16[1,4,32,2048]{3,2,0,1:T(8,128)(2,1)} %reduce-scatter.3.cloned.1.call-done), channel_id=1, replica_groups=mesh['sp'=4,'tp'=8] {'sp'}, dimensions={1} | all-to-all | bytes 1048576 | tf_op jit(solution)/shard_map/all_to_all | solution.py:94
  251.4 7.5 %fusion.10 = bf16[1,2048,768]{2,1,0:T(8,128)(2,1)} fusion(bf16[1024,2048]{1,0:T(8,128)(2,1)} %bitcast.106, bf16[1024,768]{1,0:T(8,128)(2,1)S(1)} %copy-done.47), kind=kOutput, calls=%fused_computation.55 | convolution fusion | flops 3222798336 | bytes 8912896 | tf_op jit(solution)/shard_map/dot_general | solution.py:17
  258.9 7.3 %fusion.11 = bf16[1,768,2048]{2,1,0:T(8,128)(2,1)} fusion(bf16[1024,2048]{1,0:T(8,128)(2,1)} %bitcast.6, f32[1024,768]{1,0:T(8,128)S(1)} %copy-done.44, f32[1024,768]{1,0:T(8,128)S(1)} %copy-done.43), kind=kOutput, calls=%fused_computation.56 | convolution fusion | flops 3227516928 | bytes 13631488 | tf_op jit(solution)/shard_map/dot_general | solution.py:17
  266.2 29.7 %all-gather.3.cloned.1.call-done = bf16[1,4,256,2048]{3,2,0,1:T(8,128)(2,1)} async-done(((bf16[1,4,32,2048]{3,2,0,1:T(8,128)(2,1)}), bf16[1,4,256,2048]{3,2,0,1:T(8,128)(2,1)}) %all-gather.3.cloned.1.call-update) | async-done | bytes 4194320 | tf_op jit(solution)/shard_map/all_gather | solution.py:97
  295.9 6.5 %bitcast_convert_fusion = f32[1024,2048]{1,0:T(8,128)} fusion(bf16[1,4,256,2048]{3,2,0,1:T(8,128)(2,1)} %all-gather.3.cloned.1.call-done), kind=kLoop, calls=%fused_computation.5 | loop fusion | flops 2097152 | bytes 12582912 | tf_op jit(solution)/shard_map/reshape | solution.py:100
  302.4 8.8 %gather_fusion.2 = f32[512,2048]{1,0:T(8,128)} fusion(f32[1024,2048]{1,0:T(8,128)} %bitcast_convert_fusion, s32[1024]{0:T(1024)S(1)} %pad_clamp_fusion), kind=kCustom, calls=%fused_computation.2 | custom fusion | bytes 8390656 | tf_op jit(solution)/shard_map/gather | solution.py:100
  311.2 5.8 %reshape.157 = f32[256,2,2048]{2,1,0:T(2,128)} reshape(f32[512,2048]{1,0:T(8,128)} %gather_fusion.2) | data formatting | bytes 8388608 | tf_op jit(solution)/shard_map/reshape | solution.py:100
  317.0 7.3 %reduce_sum.40 = f32[256,2048]{1,0:T(8,128)S(1)} reduce(f32[256,2,2048]{2,1,0:T(2,128)} %reshape.157, f32[]{:T(128)} %constant.43.clone.1), dimensions={1}, to_apply=%region_5.6 | reduce | flops 524288 | bytes 6291460 | tf_op jit(solution)/shard_map/reduce_sum | solution.py:101
  324.4 1.7 convolution_convert_fusion.3
  326.1 3.0 fusion.121
  329.1 14.7 %all-reduce = (f32[256]{0:T(256)S(1)}, f32[256]{0:T(256)S(1)}) all-reduce(f32[256]{0:T(256)} %get-tuple-element.25, f32[256]{0:T(256)} %get-tuple-element.24), channel_id=1, replica_groups=mesh['sp'=4,'tp'=8] {'tp'}, use_global_device_ids=true, to_apply=%region_10.11 | all-reduce | flops 512 | bytes 4096 | tf_op jit(solution)/shard_map/psum | solution.py:115
  345.2 3.5 collective-permute-start
  348.8 8.0 %fusion.9 = bf16[1,2048,768]{2,1,0:T(8,128)(2,1)} fusion(bf16[1024,2048]{1,0:T(8,128)(2,1)} %bitcast.107, bf16[1024,768]{1,0:T(8,128)(2,1)} %copy-done.45), kind=kOutput, calls=%fused_computation.54 | convolution fusion | flops 3222798336 | bytes 8912896 | tf_op jit(solution)/shard_map/dot_general | solution.py:17
  357.1 2.1 multiply_convert_fusion.5
  361.8 1.8 convert_element_type.95
  (134 shorter events, 9.8 us)
Async XLA Ops:
  7.2 106.1 %copy-start = (bf16[1,2048,768]{2,1,0:T(8,128)(2,1)S(1)}, bf16[1,2048,768]{2,1,0:T(8,128)(2,1)}, u32[]{:S(2)}) copy-start(bf16[1,2048,768]{2,1,0:T(8,128)(2,1)} %param.19) | copy-start | bytes 9437188
  107.0 51.6 %all-to-all-start.1 = ((bf16[4,256,2048]{2,1,0:T(8,128)(2,1)}), bf16[4,256,2048]{2,1,0:T(8,128)(2,1)}, u32[]{:S(2)}, u32[]{:S(2)}) async-start(bf16[4,256,2048]{2,1,0:T(8,128)(2,1)} %get-tuple-element.65), calls=%async_computation.1 | async-start | bytes 8388608 | tf_op jit(solution)/shard_map/all_to_all | solution.py:82
  112.9 125.9 %reduce-scatter.3.cloned.1.call-start = ((), (), s32[]{:S(2)}) async-start(), calls=%async_computation.5 | async-start | bytes 4718592 | tf_op jit(solution)/shard_map/reduce_scatter | solution.py:91
  188.4 61.3 %copy-start.4 = (bf16[256,256]{1,0:T(8,128)(2,1)S(1)}, bf16[256,256]{1,0:T(8,128)(2,1)}, u32[]{:S(2)}) copy-start(bf16[256,256]{1,0:T(8,128)(2,1)} %param.27) | copy-start | bytes 393220
  188.4 61.4 %copy-start.5 = (bf16[256,256]{1,0:T(8,128)(2,1)S(1)}, bf16[256,256]{1,0:T(8,128)(2,1)}, u32[]{:S(2)}) copy-start(bf16[256,256]{1,0:T(8,128)(2,1)} %param.26) | copy-start | bytes 393220
  188.4 61.5 %copy-start.6 = (bf16[256,256]{1,0:T(8,128)(2,1)S(1)}, bf16[256,256]{1,0:T(8,128)(2,1)}, u32[]{:S(2)}) copy-start(bf16[256,256]{1,0:T(8,128)(2,1)} %param.25) | copy-start | bytes 393220
  188.4 61.6 %copy-start.7 = (f32[31,256]{1,0:T(8,128)S(1)}, f32[31,256]{1,0:T(8,128)}, u32[]{:S(2)}) copy-start(f32[31,256]{1,0:T(8,128)} %param.24) | copy-start | bytes 95236
  188.4 62.9 %copy-start.47 = (bf16[1024,768]{1,0:T(8,128)(2,1)S(1)}, bf16[1024,768]{1,0:T(8,128)(2,1)}, u32[]{:S(2)}) copy-start(bf16[1024,768]{1,0:T(8,128)(2,1)} %copy-done.46) | copy-start | bytes 4718596
  188.5 107.4 %all-gather.3.cloned.1.call-start = ((), (), s32[]{:S(2)}) async-start(), calls=%async_computation.7 | async-start | bytes 4718592 | tf_op jit(solution)/shard_map/all_gather | solution.py:97
  249.6 112.1 %reduce-scatter.5.cloned.1.call-start = ((), (), s32[]{:S(2)}) async-start(), calls=%async_computation.6 | async-start | bytes 1310720 | tf_op jit(solution)/shard_map/reduce_scatter | solution.py:107
  344.9 11.9 %copy-start.11 = (f32[1,256]{1,0:T(1,128)S(1)}, f32[1,256]{1,0:T(1,128)}, u32[]{:S(2)}) copy-start(f32[1,256]{1,0:T(1,128)} %get-tuple-element.52) | copy-start | bytes 3076
  344.9 11.9 %copy-start.12 = (f32[1,256]{1,0:T(1,128)S(1)}, f32[1,256]{1,0:T(1,128)}, u32[]{:S(2)}) copy-start(f32[1,256]{1,0:T(1,128)} %get-tuple-element.53) | copy-start | bytes 3076
  344.9 11.9 %copy-start.13 = (f32[1,256]{1,0:T(1,128)S(1)}, f32[1,256]{1,0:T(1,128)}, u32[]{:S(2)}) copy-start(f32[1,256]{1,0:T(1,128)} %get-tuple-element.54) | copy-start | bytes 3076
  345.0 11.9 %copy-start.14 = (f32[1,256]{1,0:T(1,128)S(1)}, f32[1,256]{1,0:T(1,128)}, u32[]{:S(2)}) copy-start(f32[1,256]{1,0:T(1,128)} %get-tuple-element.55) | copy-start | bytes 3076
  345.0 11.9 %copy-start.15 = (f32[1,256]{1,0:T(1,128)S(1)}, f32[1,256]{1,0:T(1,128)}, u32[]{:S(2)}) copy-start(f32[1,256]{1,0:T(1,128)} %get-tuple-element.56) | copy-start | bytes 3076
  345.0 11.9 %copy-start.16 = (f32[1,256]{1,0:T(1,128)S(1)}, f32[1,256]{1,0:T(1,128)}, u32[]{:S(2)}) copy-start(f32[1,256]{1,0:T(1,128)} %get-tuple-element.57) | copy-start | bytes 3076
  345.0 11.9 %copy-start.17 = (f32[1,256]{1,0:T(1,128)S(1)}, f32[1,256]{1,0:T(1,128)}, u32[]{:S(2)}) copy-start(f32[1,256]{1,0:T(1,128)} %get-tuple-element.58) | copy-start | bytes 3076
  345.0 11.9 %copy-start.18 = (f32[1,256]{1,0:T(1,128)S(1)}, f32[1,256]{1,0:T(1,128)}, u32[]{:S(2)}) copy-start(f32[1,256]{1,0:T(1,128)} %get-tuple-element.59) | copy-start | bytes 3076
  345.0 11.9 %copy-start.19 = (f32[1,256]{1,0:T(1,128)S(1)}, f32[1,256]{1,0:T(1,128)}, u32[]{:S(2)}) copy-start(f32[1,256]{1,0:T(1,128)} %get-tuple-element.60) | copy-start | bytes 3076
  345.0 11.9 %copy-start.20 = (f32[1,256]{1,0:T(1,128)S(1)}, f32[1,256]{1,0:T(1,128)}, u32[]{:S(2)}) copy-start(f32[1,256]{1,0:T(1,128)} %get-tuple-element.61) | copy-start | bytes 3076
  345.0 11.9 %copy-start.21 = (f32[1,256]{1,0:T(1,128)S(1)}, f32[1,256]{1,0:T(1,128)}, u32[]{:S(2)}) copy-start(f32[1,256]{1,0:T(1,128)} %get-tuple-element.62) | copy-start | bytes 3076
  345.0 11.9 %copy-start.22 = (f32[1,256]{1,0:T(1,128)S(1)}, f32[1,256]{1,0:T(1,128)}, u32[]{:S(2)}) copy-start(f32[1,256]{1,0:T(1,128)} %get-tuple-element.32) | copy-start | bytes 3076
  345.0 11.9 %copy-start.23 = (f32[1,256]{1,0:T(1,128)S(1)}, f32[1,256]{1,0:T(1,128)}, u32[]{:S(2)}) copy-start(f32[1,256]{1,0:T(1,128)} %get-tuple-element.33) | copy-start | bytes 3076
  345.1 11.9 %copy-start.24 = (f32[1,256]{1,0:T(1,128)S(1)}, f32[1,256]{1,0:T(1,128)}, u32[]{:S(2)}) copy-start(f32[1,256]{1,0:T(1,128)} %get-tuple-element.34) | copy-start | bytes 3076
  345.1 11.9 %copy-start.25 = (f32[1,256]{1,0:T(1,128)S(1)}, f32[1,256]{1,0:T(1,128)}, u32[]{:S(2)}) copy-start(f32[1,256]{1,0:T(1,128)} %get-tuple-element.35) | copy-start | bytes 3076
  345.1 11.9 %copy-start.26 = (f32[1,256]{1,0:T(1,128)S(1)}, f32[1,256]{1,0:T(1,128)}, u32[]{:S(2)}) copy-start(f32[1,256]{1,0:T(1,128)} %get-tuple-element.36) | copy-start | bytes 3076
  345.1 11.9 %copy-start.27 = (f32[1,256]{1,0:T(1,128)S(1)}, f32[1,256]{1,0:T(1,128)}, u32[]{:S(2)}) copy-start(f32[1,256]{1,0:T(1,128)} %get-tuple-element.37) | copy-start | bytes 3076
  345.1 11.9 %copy-start.28 = (f32[1,256]{1,0:T(1,128)S(1)}, f32[1,256]{1,0:T(1,128)}, u32[]{:S(2)}) copy-start(f32[1,256]{1,0:T(1,128)} %get-tuple-element.38) | copy-start | bytes 3076
  345.1 11.9 %copy-start.29 = (f32[1,256]{1,0:T(1,128)S(1)}, f32[1,256]{1,0:T(1,128)}, u32[]{:S(2)}) copy-start(f32[1,256]{1,0:T(1,128)} %get-tuple-element.39) | copy-start | bytes 3076
  345.1 11.9 %copy-start.30 = (f32[1,256]{1,0:T(1,128)S(1)}, f32[1,256]{1,0:T(1,128)}, u32[]{:S(2)}) copy-start(f32[1,256]{1,0:T(1,128)} %get-tuple-element.40) | copy-start | bytes 3076
  345.2 11.6 %collective-permute-start = (f32[256,30]{0,1:T(8,128)S(1)}, f32[256,30]{0,1:T(8,128)S(1)}, u32[]{:S(2)}, u32[]{:S(2)}) collective-permute-start(f32[256,30]{0,1:T(8,128)S(1)} %slice.263), channel_id=1, source_target_pairs={{8,0},{16,8},{24,16},{9,1},{17,9},{25,17},{10,2},{18,10},{26,18},{... | collective-permute-start | bytes 92168 | tf_op jit(solution)/shard_map/ppermute | solution.py:13
  348.8 14.8 %copy-start.1 = (bf16[1,2048,768]{2,1,0:T(8,128)(2,1)S(1)}, bf16[1,2048,768]{2,1,0:T(8,128)(2,1)}, u32[]{:S(2)}) copy-start(bf16[1,2048,768]{2,1,0:T(8,128)(2,1)} %param.19) | copy-start | bytes 9437188
  (21 other events, 188.6 us)
Sparse Core Ops, SparseCore 0:
  188.6 50.2 reduce-scatter.2
  249.7 46.1 all-gather.2
  326.2 27.0 reduce-scatter.4
where the time goes:
time: 377 us; the launch traced here: 370 us
  waiting for transfers between devices  113 us (30%)
  blocking collectives  76.3 us (20%)
  matrix products  69.8 us (19%)
  local copies, waits for them, and re-layouts  55.4 us (15%)
  other arithmetic  31.3 us (8%)
  between operations  14.8 us (4%)
  starting transfers between devices  9.92 us (3%)
    dot_general x8, matrix products, contract(): lax.dot_general(left, right, (((left_dim,), (right_dim,)), ((), ())), pre...  57.3 us
    all_to_all x1, blocking collectives, on_device(): lax.all_to_all(send_in, 'sp', split_axis=0, concat_axis=1, tiled=True)  50.8 us
    reduce_scatter x1, waiting for transfers between devices, on_device(): lax.psum_scatter(blocks.astype(jnp.bfloat16), 'tp', scatter_dimension=2,...  50.3 us
    all_to_all x1, waiting for transfers between devices, on_device(): lax.all_to_all(send_cot, 'sp', split_axis=0, concat_axis=1, tiled=True)  32.8 us
    all_gather x1, waiting for transfers between devices, on_device(): lax.all_gather(returned.astype(jnp.bfloat16), 'tp', axis=2, tiled=True)  29.7 us
    psum x1, blocking collectives, on_device(): lax.psum((jnp.sum(norm_cot, axis=0), jnp.sum(norm_cot * centered, axis=0)...  14.7 us
    mul x3, local copies, waits for them, and re-layouts, on_device(): route_weight[:, :, None] * cotangent.astype(jnp.float32)[:, None, :]  11.6 us
    all_to_all x1, blocking collectives, on_device(): lax.all_to_all(share.astype(jnp.bfloat16), 'sp', split_axis=1, concat_axi...  10.8 us
  transfers between devices with their start and end apart: 5, of which 3 were waited for; matrix products, arithmetic and copies ran while one was open for 12% of the time, Pallas kernels for 0%

commit v1 on v0

--- a/solution.py
+++ b/solution.py
@@ -5,6 +5,11 @@
 
 D = 2048
 C = 2048
+
+
+def gathered_along(shard, axis, along):
+    parts = lax.all_gather(shard, axis)
+    return jnp.concatenate(parts, axis=along)
 
 
 def from_behind(value, axis, by):
@@ -94,9 +99,7 @@
     returned = lax.all_to_all(
         share.astype(jnp.bfloat16), "sp", split_axis=1, concat_axis=0, tiled=True
     ).astype(share.dtype)
-    whole = lax.all_gather(returned.astype(jnp.bfloat16), "tp", axis=2, tiled=True).astype(
-        returned.dtype
-    )
+    whole = gathered_along(returned.astype(jnp.bfloat16), "tp", 2).astype(returned.dtype)
     routed = whole.reshape(expert_count * capacity, D)[target].reshape(tokens_here, 2, D)
     summed = jnp.sum(routed, axis=1)
     mixed_cot = (cotangent.astype(jnp.float32) + summed).astype(jnp.bfloat16)

time: 377 us -> 363 us (0.963)
  matrix products: 69.8 us -> 57.9 us
  other arithmetic: 31.3 us -> 26.3 us
    dot_general x8, matrix products: 57.3 us -> 45.4 us  [contract(): lax.dot_general(left, right, (((left_dim,), (right_dim,)), ((), ())), pre...]
    reshape x1 -> x0, other arithmetic: 6.54 us -> none  [on_device(): whole.reshape(expert_count * capacity, D)[target].reshape(tokens_here, 2, D)]
    convert_element_type x0 -> x1, local copies, waits for them, and re-layouts: none -> 3.86 us  [on_device(): gathered_along(returned.astype(jnp.bfloat16), 'tp', 2)]
where the time goes in v1:
time: 363 us; the launch traced here: 357 us
  waiting for transfers between devices  113 us (31%)
  blocking collectives  76.3 us (21%)
  local copies, waits for them, and re-layouts  58.8 us (16%)
  matrix products  57.9 us (16%)
  other arithmetic  26.3 us (7%)
  between operations  14.9 us (4%)
  starting transfers between devices  9.82 us (3%)
    all_to_all x1, blocking collectives, on_device(): lax.all_to_all(send_in, 'sp', split_axis=0, concat_axis=1, tiled=True)  50.8 us
    reduce_scatter x1, waiting for transfers between devices, on_device(): lax.psum_scatter(blocks.astype(jnp.bfloat16), 'tp', scatter_dimension=2,...  50.3 us
    dot_general x8, matrix products, contract(): lax.dot_general(left, right, (((left_dim,), (right_dim,)), ((), ())), pre...  45.4 us
    all_to_all x1, waiting for transfers between devices, on_device(): lax.all_to_all(send_cot, 'sp', split_axis=0, concat_axis=1, tiled=True)  32.7 us
    all_gather x1, waiting for transfers between devices, gathered_along(): parts = lax.all_gather(shard, axis)  29.7 us
    psum x1, blocking collectives, on_device(): lax.psum((jnp.sum(norm_cot, axis=0), jnp.sum(norm_cot * centered, axis=0)...  14.7 us
    mul x3, local copies, waits for them, and re-layouts, on_device(): route_weight[:, :, None] * cotangent.astype(jnp.float32)[:, None, :]  11.6 us
    all_to_all x1, blocking collectives, on_device(): lax.all_to_all(share.astype(jnp.bfloat16), 'sp', split_axis=1, concat_axi...  10.8 us
  transfers between devices with their start and end apart: 5, of which 3 were waited for; matrix products, arithmetic and copies ran while one was open for 12% of the time, Pallas kernels for 0%

profile of v1, /device:TPU:4, one launch (start us, length us, event | category | flops | bytes accessed | tf_op | source)
XLA Modules:
  0.0 356.7 jit_solution(5410079144028633634)
XLA Ops:
  11.3 2.4 scatter_custom_fusion
  13.8 5.3 %mul.440 = f32[256,2,2048]{2,1,0:T(2,128)} broadcast(bf16[256,2048]{1,0:T(8,128)(2,1)} %param.16), dimensions={0,2} | broadcast | bytes 5242880 | tf_op jit(solution)/shard_map/mul | solution.py:77
  19.1 6.2 %mul.441 = f32[512,2048]{1,0:T(8,128)} reshape(f32[256,2,2048]{2,1,0:T(2,128)} %mul.440) | data formatting | bytes 8388608 | tf_op jit(solution)/shard_map/mul | solution.py:77
  25.6 3.8 %multiply_convert_fusion = bf16[512,2048]{1,0:T(8,128)(2,1)} fusion(f32[512,2048]{1,0:T(8,128)} %mul.441, f32[512]{0:T(512)S(1)} %mul.438), kind=kLoop, calls=%fused_computation.6 | loop fusion | flops 2097152 | bytes 6293504 | tf_op jit(solution)/shard_map/convert_element_type | solution.py:77
  29.4 10.7 %gather_fusion.1 = bf16[1024,2048]{1,0:T(8,128)(2,1)} fusion(bf16[512,2048]{1,0:T(8,128)(2,1)} %multiply_convert_fusion, s32[1024]{0:T(1024)S(1)} %get-tuple-element.63), kind=kCustom, calls=%fused_computation.1 | custom fusion | bytes 8392704 | tf_op jit(solution)/shard_map/gather | solution.py:81
  40.1 10.2 %gather_fusion = bf16[1024,2048]{1,0:T(8,128)(2,1)} fusion(bf16[256,2048]{1,0:T(8,128)(2,1)} %param.15, s32[1024]{0:T(1024)S(1)} %get-tuple-element.64), kind=kCustom, calls=%fused_computation | custom fusion | bytes 8392704 | tf_op jit(solution)/shard_map/gather | solution.py:84
  50.3 5.2 %broadcast_select_fusion = (bf16[4,256,2048]{2,1,0:T(8,128)(2,1)}, bf16[4,256,2048]{2,1,0:T(8,128)(2,1)S(1)}) fusion(bf16[4,256,2048]{2,1,0:T(8,128)(2,1)} %bitcast.107, pred[4,256]{1,0:T(4,128)(4,1)S(1)} %broadcast_in_dim.43, bf16[4,256,2048]{2,1,0:T(8,128)(2,1)} %bitcast.108), kind=kLoop, calls=%fused_computation.7 | loop fusion | flops 4194304 | bytes 16778240 | tf_op jit(solution)/shard_map/jit(_where)/select_n | solution.py:81
  55.4 50.8 %all_to_all.30 = bf16[4,256,2048]{2,1,0:T(8,128)(2,1)} all-to-all(bf16[4,256,2048]{2,1,0:T(8,128)(2,1)S(1)} %get-tuple-element.66), channel_id=1, replica_groups=mesh['sp'=4,'tp'=8] {'sp'}, dimensions={0} | all-to-all | bytes 8388608 | tf_op jit(solution)/shard_map/all_to_all | solution.py:88
  106.3 5.9 %all-to-all-start.1 = ((bf16[4,256,2048]{2,1,0:T(8,128)(2,1)}), bf16[4,256,2048]{2,1,0:T(8,128)(2,1)}, u32[]{:S(2)}, u32[]{:S(2)}) async-start(bf16[4,256,2048]{2,1,0:T(8,128)(2,1)} %get-tuple-element.65), calls=%async_computation.1 | async-start | bytes 8388608 | tf_op jit(solution)/shard_map/all_to_all | solution.py:87
  112.7 7.4 %fusion.2 = f32[1024,768]{1,0:T(8,128)} fusion(bf16[1024,2048]{1,0:T(8,128)(2,1)} %bitcast.109, bf16[1,2048,768]{2,1,0:T(8,128)(2,1)S(1)} %copy-done), kind=kOutput, calls=%fused_computation.43 | convolution fusion | flops 3221225472 | bytes 10485760 | tf_op jit(solution)/shard_map/dot_general | solution.py:28
  120.1 5.1 %fusion.5 = f32[1024,768]{1,0:T(8,128)} fusion(bf16[1024,2048]{1,0:T(8,128)(2,1)S(1)} %bitcast.112, bf16[1,2048,768]{2,1,0:T(8,128)(2,1)S(1)} %copy-done.42), kind=kOutput, calls=%fused_computation.46 | convolution fusion | flops 3221225472 | bytes 10485760 | tf_op jit(solution)/shard_map/dot_general | solution.py:29
  125.2 32.7 %all-to-all-done.1 = bf16[4,256,2048]{2,1,0:T(8,128)(2,1)} async-done(((bf16[4,256,2048]{2,1,0:T(8,128)(2,1)}), bf16[4,256,2048]{2,1,0:T(8,128)(2,1)}, u32[]{:S(2)}, u32[]{:S(2)}) %all-to-all-start.1) | async-done | bytes 4194336 | tf_op jit(solution)/shard_map/all_to_all | solution.py:87
  157.9 9.2 %multiply_convert_fusion.2 = (bf16[1024,768]{1,0:T(8,128)(2,1)S(1)}, bf16[1024,768]{1,0:T(8,128)(2,1)S(1)}) fusion(f32[1024,768]{1,0:T(8,128)} %fusion.2, f32[1024,768]{1,0:T(8,128)} %fusion.5, bf16[1024,2048]{1,0:T(8,128)(2,1)} %bitcast.6, bf16[1,768,2048]{2,1,0:T(8,128)(2,1)} %param.21), kind=kOutput, calls=%fused_computation.51 | convolution fusion | flops 3231449088 | bytes 16777216 | tf_op jit(solution)/shard_map/dot_general | solution.py:22
  167.1 3.4 fusion
  170.6 5.2 %add_convert_fusion = bf16[1024,2048]{1,0:T(8,128)(2,1)} fusion(f32[1024,2048]{1,0:T(8,128)S(1)} %fusion, bf16[1024,768]{1,0:T(8,128)(2,1)S(1)} %get-tuple-element.30, bf16[1,2048,768]{2,1,0:T(8,128)(2,1)S(1)} %copy-done.43), kind=kOutput, calls=%fused_computation.5 | convolution fusion | flops 3225419776 | bytes 17301504 | tf_op jit(solution)/shard_map/dot_general | solution.py:22
  175.9 50.3 %reduce-scatter.3.cloned.1.call-done = bf16[1,4,32,2048]{3,2,0,1:T(8,128)(2,1)} async-done(((bf16[1,4,256,2048]{3,2,0,1:T(8,128)(2,1)}), bf16[1,4,32,2048]{3,2,0,1:T(8,128)(2,1)}) %reduce-scatter.3.cloned.1.call-update) | async-done | bytes 524304 | tf_op jit(solution)/shard_map/reduce_scatter | solution.py:96
  226.2 10.8 %all_to_all.31 = bf16[1,4,32,2048]{3,2,0,1:T(8,128)(2,1)} all-to-all(bf16[1,4,32,2048]{3,2,0,1:T(8,128)(2,1)} %reduce-scatter.3.cloned.1.call-done), channel_id=1, replica_groups=mesh['sp'=4,'tp'=8] {'sp'}, dimensions={1} | all-to-all | bytes 1048576 | tf_op jit(solution)/shard_map/all_to_all | solution.py:99
  238.8 7.5 %fusion.9 = bf16[1,2048,768]{2,1,0:T(8,128)(2,1)} fusion(bf16[1024,2048]{1,0:T(8,128)(2,1)} %bitcast.110, bf16[1024,768]{1,0:T(8,128)(2,1)S(1)} %copy-done.47), kind=kOutput, calls=%fused_computation.54 | convolution fusion | flops 3222798336 | bytes 8912896 | tf_op jit(solution)/shard_map/dot_general | solution.py:22
  246.3 7.3 %fusion.11 = bf16[1,768,2048]{2,1,0:T(8,128)(2,1)} fusion(bf16[1024,2048]{1,0:T(8,128)(2,1)} %bitcast.6, f32[1024,768]{1,0:T(8,128)S(1)} %copy-done.45, f32[1024,768]{1,0:T(8,128)S(1)} %copy-done.44), kind=kOutput, calls=%fused_computation.56 | convolution fusion | flops 3227516928 | bytes 13631488 | tf_op jit(solution)/shard_map/dot_general | solution.py:22
  253.6 29.7 %all-gather.3.cloned.1.call-done = bf16[8,4,32,2048]{3,2,1,0:T(8,128)(2,1)} async-done(((bf16[1,4,32,2048]{3,2,1,0:T(8,128)(2,1)}), bf16[8,4,32,2048]{3,2,1,0:T(8,128)(2,1)}) %all-gather.3.cloned.1.call-update) | async-done | bytes 4194320 | tf_op jit(solution)/shard_map/all_gather | solution.py:11
  283.3 3.2 convert_bitcast_fusion
  286.5 3.9 %copy.43 = f32[4,1,8,32,2048]{4,3,2,0,1:T(8,128)} copy(f32[4,1,8,32,2048]{4,3,0,2,1:T(8,128)S(1)} %convert_bitcast_fusion) | data formatting | bytes 16777216 | tf_op jit(solution)/shard_map/convert_element_type | solution.py:102
  290.4 8.8 %gather_fusion.2 = f32[512,2048]{1,0:T(8,128)} fusion(f32[1024,2048]{1,0:T(8,128)} %bitcast.106, s32[1024]{0:T(1024)S(1)} %pad_clamp_fusion), kind=kCustom, calls=%fused_computation.2 | custom fusion | bytes 8390656 | tf_op jit(solution)/shard_map/gather | solution.py:103
  299.1 6.0 %reshape.158 = f32[256,2,2048]{2,1,0:T(2,128)} reshape(f32[512,2048]{1,0:T(8,128)} %gather_fusion.2) | data formatting | bytes 8388608 | tf_op jit(solution)/shard_map/reshape | solution.py:103
  305.2 7.3 %reduce_sum.40 = f32[256,2048]{1,0:T(8,128)S(1)} reduce(f32[256,2,2048]{2,1,0:T(2,128)} %reshape.158, f32[]{:T(128)} %constant.43.clone.1), dimensions={1}, to_apply=%region_5.6 | reduce | flops 524288 | bytes 6291460 | tf_op jit(solution)/shard_map/reduce_sum | solution.py:104
  312.5 1.7 convolution_convert_fusion.3
  314.3 3.0 fusion.121
  317.2 14.7 %all-reduce = (f32[256]{0:T(256)S(1)}, f32[256]{0:T(256)S(1)}) all-reduce(f32[256]{0:T(256)} %get-tuple-element.25, f32[256]{0:T(256)} %get-tuple-element.24), channel_id=1, replica_groups=mesh['sp'=4,'tp'=8] {'tp'}, use_global_device_ids=true, to_apply=%region_10.11 | all-reduce | flops 512 | bytes 4096 | tf_op jit(solution)/shard_map/psum | solution.py:118
  333.4 3.4 collective-permute-start
  336.8 8.0 %fusion.10 = bf16[1,2048,768]{2,1,0:T(8,128)(2,1)} fusion(bf16[1024,2048]{1,0:T(8,128)(2,1)} %bitcast.111, bf16[1024,768]{1,0:T(8,128)(2,1)} %copy-done.48), kind=kOutput, calls=%fused_computation.55 | convolution fusion | flops 3222798336 | bytes 8912896 | tf_op jit(solution)/shard_map/dot_general | solution.py:22
  345.1 1.5 multiply_convert_fusion.5
  348.2 1.8 convert_element_type.109
  (137 shorter events, 9.6 us)
Async XLA Ops:
  7.2 105.5 %copy-start = (bf16[1,2048,768]{2,1,0:T(8,128)(2,1)S(1)}, bf16[1,2048,768]{2,1,0:T(8,128)(2,1)}, u32[]{:S(2)}) copy-start(bf16[1,2048,768]{2,1,0:T(8,128)(2,1)} %param.19) | copy-start | bytes 9437188
  106.3 51.6 %all-to-all-start.1 = ((bf16[4,256,2048]{2,1,0:T(8,128)(2,1)}), bf16[4,256,2048]{2,1,0:T(8,128)(2,1)}, u32[]{:S(2)}, u32[]{:S(2)}) async-start(bf16[4,256,2048]{2,1,0:T(8,128)(2,1)} %get-tuple-element.65), calls=%async_computation.1 | async-start | bytes 8388608 | tf_op jit(solution)/shard_map/all_to_all | solution.py:87
  112.2 114.0 %reduce-scatter.3.cloned.1.call-start = ((), (), s32[]{:S(2)}) async-start(), calls=%async_computation.5 | async-start | bytes 4718592 | tf_op jit(solution)/shard_map/reduce_scatter | solution.py:96
  175.8 61.3 %copy-start.4 = (bf16[256,256]{1,0:T(8,128)(2,1)S(1)}, bf16[256,256]{1,0:T(8,128)(2,1)}, u32[]{:S(2)}) copy-start(bf16[256,256]{1,0:T(8,128)(2,1)} %param.27) | copy-start | bytes 393220
  175.8 61.4 %copy-start.5 = (bf16[256,256]{1,0:T(8,128)(2,1)S(1)}, bf16[256,256]{1,0:T(8,128)(2,1)}, u32[]{:S(2)}) copy-start(bf16[256,256]{1,0:T(8,128)(2,1)} %param.25) | copy-start | bytes 393220
  175.8 61.5 %copy-start.6 = (bf16[256,256]{1,0:T(8,128)(2,1)S(1)}, bf16[256,256]{1,0:T(8,128)(2,1)}, u32[]{:S(2)}) copy-start(bf16[256,256]{1,0:T(8,128)(2,1)} %param.26) | copy-start | bytes 393220
  175.8 61.6 %copy-start.7 = (f32[31,256]{1,0:T(8,128)S(1)}, f32[31,256]{1,0:T(8,128)}, u32[]{:S(2)}) copy-start(f32[31,256]{1,0:T(8,128)} %param.24) | copy-start | bytes 95236
  175.8 62.9 %copy-start.47 = (bf16[1024,768]{1,0:T(8,128)(2,1)S(1)}, bf16[1024,768]{1,0:T(8,128)(2,1)}, u32[]{:S(2)}) copy-start(bf16[1024,768]{1,0:T(8,128)(2,1)} %copy-done.46) | copy-start | bytes 4718596
  175.8 107.4 %all-gather.3.cloned.1.call-start = ((), (), s32[]{:S(2)}) async-start(), calls=%async_computation.7 | async-start | bytes 4718592 | tf_op jit(solution)/shard_map/all_gather | solution.py:11
  237.0 111.1 %reduce-scatter.5.cloned.1.call-start = ((), (), s32[]{:S(2)}) async-start(), calls=%async_computation.6 | async-start | bytes 1310720 | tf_op jit(solution)/shard_map/reduce_scatter | solution.py:110
  333.1 11.7 %copy-start.11 = (f32[1,256]{1,0:T(1,128)S(1)}, f32[1,256]{1,0:T(1,128)}, u32[]{:S(2)}) copy-start(f32[1,256]{1,0:T(1,128)} %get-tuple-element.52) | copy-start | bytes 3076
  333.1 11.7 %copy-start.12 = (f32[1,256]{1,0:T(1,128)S(1)}, f32[1,256]{1,0:T(1,128)}, u32[]{:S(2)}) copy-start(f32[1,256]{1,0:T(1,128)} %get-tuple-element.53) | copy-start | bytes 3076
  333.1 11.7 %copy-start.13 = (f32[1,256]{1,0:T(1,128)S(1)}, f32[1,256]{1,0:T(1,128)}, u32[]{:S(2)}) copy-start(f32[1,256]{1,0:T(1,128)} %get-tuple-element.54) | copy-start | bytes 3076
  333.1 11.7 %copy-start.14 = (f32[1,256]{1,0:T(1,128)S(1)}, f32[1,256]{1,0:T(1,128)}, u32[]{:S(2)}) copy-start(f32[1,256]{1,0:T(1,128)} %get-tuple-element.55) | copy-start | bytes 3076
  333.1 11.7 %copy-start.15 = (f32[1,256]{1,0:T(1,128)S(1)}, f32[1,256]{1,0:T(1,128)}, u32[]{:S(2)}) copy-start(f32[1,256]{1,0:T(1,128)} %get-tuple-element.56) | copy-start | bytes 3076
  333.1 11.7 %copy-start.16 = (f32[1,256]{1,0:T(1,128)S(1)}, f32[1,256]{1,0:T(1,128)}, u32[]{:S(2)}) copy-start(f32[1,256]{1,0:T(1,128)} %get-tuple-element.57) | copy-start | bytes 3076
  333.2 11.7 %copy-start.17 = (f32[1,256]{1,0:T(1,128)S(1)}, f32[1,256]{1,0:T(1,128)}, u32[]{:S(2)}) copy-start(f32[1,256]{1,0:T(1,128)} %get-tuple-element.58) | copy-start | bytes 3076
  333.2 11.7 %copy-start.18 = (f32[1,256]{1,0:T(1,128)S(1)}, f32[1,256]{1,0:T(1,128)}, u32[]{:S(2)}) copy-start(f32[1,256]{1,0:T(1,128)} %get-tuple-element.59) | copy-start | bytes 3076
  333.2 11.7 %copy-start.19 = (f32[1,256]{1,0:T(1,128)S(1)}, f32[1,256]{1,0:T(1,128)}, u32[]{:S(2)}) copy-start(f32[1,256]{1,0:T(1,128)} %get-tuple-element.60) | copy-start | bytes 3076
  333.2 11.7 %copy-start.20 = (f32[1,256]{1,0:T(1,128)S(1)}, f32[1,256]{1,0:T(1,128)}, u32[]{:S(2)}) copy-start(f32[1,256]{1,0:T(1,128)} %get-tuple-element.61) | copy-start | bytes 3076
  333.2 11.7 %copy-start.21 = (f32[1,256]{1,0:T(1,128)S(1)}, f32[1,256]{1,0:T(1,128)}, u32[]{:S(2)}) copy-start(f32[1,256]{1,0:T(1,128)} %get-tuple-element.62) | copy-start | bytes 3076
  333.2 11.7 %copy-start.22 = (f32[1,256]{1,0:T(1,128)S(1)}, f32[1,256]{1,0:T(1,128)}, u32[]{:S(2)}) copy-start(f32[1,256]{1,0:T(1,128)} %get-tuple-element.32) | copy-start | bytes 3076
  333.2 11.7 %copy-start.23 = (f32[1,256]{1,0:T(1,128)S(1)}, f32[1,256]{1,0:T(1,128)}, u32[]{:S(2)}) copy-start(f32[1,256]{1,0:T(1,128)} %get-tuple-element.33) | copy-start | bytes 3076
  333.2 11.7 %copy-start.24 = (f32[1,256]{1,0:T(1,128)S(1)}, f32[1,256]{1,0:T(1,128)}, u32[]{:S(2)}) copy-start(f32[1,256]{1,0:T(1,128)} %get-tuple-element.34) | copy-start | bytes 3076
  333.2 11.7 %copy-start.25 = (f32[1,256]{1,0:T(1,128)S(1)}, f32[1,256]{1,0:T(1,128)}, u32[]{:S(2)}) copy-start(f32[1,256]{1,0:T(1,128)} %get-tuple-element.35) | copy-start | bytes 3076
  333.2 11.7 %copy-start.26 = (f32[1,256]{1,0:T(1,128)S(1)}, f32[1,256]{1,0:T(1,128)}, u32[]{:S(2)}) copy-start(f32[1,256]{1,0:T(1,128)} %get-tuple-element.36) | copy-start | bytes 3076
  333.3 11.7 %copy-start.27 = (f32[1,256]{1,0:T(1,128)S(1)}, f32[1,256]{1,0:T(1,128)}, u32[]{:S(2)}) copy-start(f32[1,256]{1,0:T(1,128)} %get-tuple-element.37) | copy-start | bytes 3076
  333.3 11.7 %copy-start.28 = (f32[1,256]{1,0:T(1,128)S(1)}, f32[1,256]{1,0:T(1,128)}, u32[]{:S(2)}) copy-start(f32[1,256]{1,0:T(1,128)} %get-tuple-element.38) | copy-start | bytes 3076
  333.3 11.7 %copy-start.29 = (f32[1,256]{1,0:T(1,128)S(1)}, f32[1,256]{1,0:T(1,128)}, u32[]{:S(2)}) copy-start(f32[1,256]{1,0:T(1,128)} %get-tuple-element.39) | copy-start | bytes 3076
  333.3 11.7 %copy-start.30 = (f32[1,256]{1,0:T(1,128)S(1)}, f32[1,256]{1,0:T(1,128)}, u32[]{:S(2)}) copy-start(f32[1,256]{1,0:T(1,128)} %get-tuple-element.40) | copy-start | bytes 3076
  333.4 11.4 %collective-permute-start = (f32[256,30]{0,1:T(8,128)S(1)}, f32[256,30]{0,1:T(8,128)S(1)}, u32[]{:S(2)}, u32[]{:S(2)}) collective-permute-start(f32[256,30]{0,1:T(8,128)S(1)} %slice.263), channel_id=1, source_target_pairs={{8,0},{16,8},{24,16},{9,1},{17,9},{25,17},{10,2},{18,10},{26,18},{... | collective-permute-start | bytes 92168 | tf_op jit(solution)/shard_map/ppermute | solution.py:18
  336.8 13.2 %copy-start.1 = (bf16[1,2048,768]{2,1,0:T(8,128)(2,1)S(1)}, bf16[1,2048,768]{2,1,0:T(8,128)(2,1)}, u32[]{:S(2)}) copy-start(bf16[1,2048,768]{2,1,0:T(8,128)(2,1)} %param.19) | copy-start | bytes 9437188
  (22 other events, 193.0 us)
Sparse Core Ops, SparseCore 0:
  176.0 50.2 reduce-scatter.2
  237.1 46.0 all-gather.2
  314.4 27.0 reduce-scatter.4
